TPU v7x, 32 devices: a whole 2x2x4 slice. The times are simulated.
32 devices in a mesh: dp: 2 (over x), kv: 8 (over z, y), tp: 2 (over core).
Axes of the slice: x: 2, y: 2, z: 4, core: 2. Of those that a mesh axis runs over, the one named last changes fastest.
Arguments:
- tokens: bfloat16 [32, 3072], P(('tp', 'dp'), 'kv'), parts along dimension 0, may hold values from -60 to 60
- old_state: float32 [32, 24, 128, 128], P(('tp', 'dp', 'kv')), parts along dimension 0, may hold values from -0.6 to 0.6
- mixer_gain: float32 [3072], replicated, may hold values from 0.1 to 1.9
- w_query: bfloat16 [3072, 3072], P(None, 'kv'), may hold values from -0.109375 to 0.109375
- w_key: bfloat16 [3072, 3072], P(None, 'kv'), may hold values from -0.109375 to 0.109375
- w_value: bfloat16 [3072, 3072], P(None, 'kv'), may hold values from -0.109375 to 0.109375
- w_outgate: bfloat16 [3072, 3072], P(None, 'kv'), may hold values from -0.109375 to 0.109375
- w_decay: bfloat16 [3072, 24], replicated, may hold values from -0.109375 to 0.109375
- w_write: bfloat16 [3072, 24], replicated, may hold values from -0.109375 to 0.109375
- decay_log: float32 [24], replicated, may hold values from -3 to 1
- decay_bias: float32 [24], replicated, may hold values from -3 to 3
- head_gain: float32 [128], replicated, may hold values from 0.1 to 1.9
- w_output: bfloat16 [3072, 3072], P('kv'), may hold values from -0.15625 to 0.15625
- channel_gain: float32 [3072], replicated, may hold values from 0.1 to 1.9
- w_gate: bfloat16 [3072, 8448], P(None, 'kv'), may hold values from -0.109375 to 0.109375
- w_up: bfloat16 [3072, 8448], P(None, 'kv'), may hold values from -0.109375 to 0.109375
- w_down: bfloat16 [8448, 3072], P(None, 'kv'), may hold values from -0.0625 to 0.0625
Outputs:
- mixed: bfloat16 [32, 3072], P(('tp', 'dp'), 'kv'), parts along dimension 0
- new_state: float32 [32, 24, 128, 128], P(('tp', 'dp', 'kv')), parts along dimension 0
There are 2 independent parts, one for each index of `tp`. A program takes and returns all parts, laid end to end along the dimension named above; an argument that names none is the same for every part. Nothing has to cross between parts.
All inputs are finite; a program needn't handle non-finite values.
Results may differ from a plain program's by a relative error of at most 0.0059.
Values may be sent and summed in bfloat16 or wider, within the bound.
A program may use at most 64 MiB of HBM per device.

v0:
```python
import jax
import jax.numpy as jnp
from jax import lax
from jax.sharding import PartitionSpec as P

HEADS = 24
HEAD_DIM = 128


EPS = 1e-06


def norm_scale(values):
    return lax.rsqrt(jnp.mean(values * values, axis=-1, keepdims=True) + EPS)


def unit_rows(values):
    return values * lax.rsqrt(jnp.sum(values * values, axis=-1, keepdims=True) + EPS)


def body(
    tokens,
    old_state,
    mixer_gain,
    w_query,
    w_key,
    w_value,
    w_outgate,
    w_decay,
    w_write,
    decay_log,
    decay_bias,
    head_gain,
    w_output,
    channel_gain,
    w_gate,
    w_up,
    w_down,
):
    local_rows = old_state.shape[0]
    width_share = tokens.shape[1]
    offset_rows = lax.axis_index("kv") * local_rows
    offset_cols = lax.axis_index("kv") * width_share
    complete_rows = lax.all_gather(tokens, "kv", axis=1, tiled=True)
    tok_wide = complete_rows.astype(jnp.float32)
    scale_in = norm_scale(tok_wide)
    normed = (tok_wide * mixer_gain).astype(jnp.bfloat16)

    def project(weight):
        return (jnp.dot(normed, weight, preferred_element_type=jnp.float32) * scale_in).astype(
            jnp.bfloat16
        )

    query_cols = project(w_query)
    key_cols = project(w_key)
    value_cols = project(w_value)
    outgate_cols = project(w_outgate)
    query_pre, key_pre, value_pre, outgate_pre = (
        lax.all_to_all(query_cols, "kv", split_axis=0, concat_axis=1, tiled=True),
        lax.all_to_all(key_cols, "kv", split_axis=0, concat_axis=1, tiled=True),
        lax.all_to_all(value_cols, "kv", split_axis=0, concat_axis=1, tiled=True),
        lax.all_to_all(outgate_cols, "kv", split_axis=0, concat_axis=1, tiled=True),
    )
    own_normed = lax.dynamic_slice_in_dim(normed, offset_rows, local_rows, 0)
    own_scale = lax.dynamic_slice_in_dim(scale_in, offset_rows, local_rows, 0)
    decay_pre = jnp.dot(own_normed, w_decay, preferred_element_type=jnp.float32) * own_scale
    write_pre = jnp.dot(own_normed, w_write, preferred_element_type=jnp.float32) * own_scale

    def by_head(values):
        return values.astype(jnp.float32).reshape(local_rows, HEADS, HEAD_DIM)

    queries = unit_rows(jax.nn.silu(by_head(query_pre))) * HEAD_DIM ** (-0.5)
    keys_unit = unit_rows(jax.nn.silu(by_head(key_pre)))
    values_act = jax.nn.silu(by_head(value_pre))
    strength = jax.nn.sigmoid(write_pre)
    retain = jnp.exp(-jnp.exp(decay_log) * jax.nn.softplus(decay_pre + decay_bias))
    recalled_values = jnp.einsum(
        "bhkv,bhk->bhv", old_state, keys_unit, precision=lax.Precision.HIGHEST
    )
    correction = values_act - retain[..., None] * recalled_values
    new_state = (
        retain[..., None, None] * old_state
        + (strength[..., None] * keys_unit)[..., :, None] * correction[..., None, :]
    )
    state_readout = jnp.einsum("bhkv,bhk->bhv", new_state, queries, precision=lax.Precision.HIGHEST)
    gated_read = (
        state_readout * norm_scale(state_readout) * head_gain * jax.nn.silu(by_head(outgate_pre))
    )
    gated_read = gated_read.reshape(local_rows, HEADS * HEAD_DIM).astype(jnp.bfloat16)
    read_cols = lax.all_to_all(gated_read, "kv", split_axis=1, concat_axis=0, tiled=True)
    partial_out = jnp.dot(read_cols, w_output, preferred_element_type=jnp.float32)
    mixer_out = lax.psum(partial_out, "kv")
    residual = lax.optimization_barrier((tok_wide + mixer_out).astype(jnp.bfloat16))
    residual_wide = residual.astype(jnp.float32)
    scale_mid = norm_scale(residual_wide)
    normed_mid = (residual_wide * channel_gain).astype(jnp.bfloat16)
    gate_act = jnp.dot(normed_mid, w_gate, preferred_element_type=jnp.float32) * scale_mid
    upward = jnp.dot(normed_mid, w_up, preferred_element_type=jnp.float32) * scale_mid
    own_residual = lax.dynamic_slice_in_dim(residual_wide, offset_cols, width_share, 1)
    hidden_units = (jax.nn.silu(gate_act) * upward).astype(jnp.bfloat16)
    down_sum = jnp.dot(
        lax.all_gather(hidden_units, "kv", axis=1, tiled=True),
        w_down,
        preferred_element_type=jnp.float32,
    )
    mixed = (own_residual + down_sum).astype(jnp.bfloat16)
    return (mixed, new_state)


def solution(mesh):
    in_specs = (
        P(("tp", "dp"), "kv"),
        P(("tp", "dp", "kv"), None, None, None),
        P(),
        P(None, "kv"),
        P(None, "kv"),
        P(None, "kv"),
        P(None, "kv"),
        P(),
        P(),
        P(),
        P(),
        P(),
        P("kv", None),
        P(),
        P(None, "kv"),
        P(None, "kv"),
        P(None, "kv"),
    )
    out_specs = (P(("tp", "dp"), "kv"), P(("tp", "dp", "kv"), None, None, None))
    return jax.shard_map(body, mesh=mesh, in_specs=in_specs, out_specs=out_specs, check_vma=False)
```

profile of v0, /device:TPU:0, one launch (start us, length us, event | category | flops | bytes accessed | tf_op | source)
XLA Modules:
  0.0 226.5 jit_solution(14168076446692269067)
XLA Ops:
  7.2 32.9 %all_gather.6 = bf16[8,3072]{1,0:T(8,128)(2,1)S(1)} all-gather(bf16[8,384]{1,0:T(8,128)(2,1)} %param.17), channel_id=1, replica_groups=mesh['dp'=2,'kv'=8,'tp'=2] {'kv'}, dimensions={1}, use_global_device_ids=true | all-gather | bytes 55296 | tf_op jit(solution)/shard_map/all_gather | solution.py:44
  40.1 0.8 fusion.24
  41.0 2.1 fusion.15
  43.0 0.5 broadcast.215
  43.6 0.6 reduce.6
  44.2 0.7 reshape.400
  44.9 5.4 %all-to-all-start = ((bf16[8,2,192]{2,1,0:T(2,128)(2,1)}), bf16[8,2,192]{2,1,0:T(2,128)(2,1)S(1)}, u32[]{:S(2)}, u32[]{:S(2)}) async-start(bf16[8,2,192]{2,1,0:T(2,128)(2,1)} %reshape.400), calls=%async_computation | async-start | bytes 16384 | tf_op jit(solution)/shard_map/all_to_all | solution.py:60
  50.3 0.6 dynamic-slice.3
  50.9 2.2 fusion.14
  53.1 0.4 fusion.13
  53.6 0.4 fusion.12
  54.0 0.1 copy-done.5
  54.1 0.8 fusion.46
  54.9 0.8 fusion.20
  55.7 0.7 reduce.7
  56.4 0.7 reshape.402
  57.1 0.6 reduce.5
  57.8 0.7 reshape.398
  58.4 0.6 reduce.4
  59.1 0.7 reshape.396
  59.8 6.0 %all-to-all-start.1 = ((bf16[8,2,192]{2,1,0:T(2,128)(2,1)}), bf16[8,2,192]{2,1,0:T(2,128)(2,1)S(1)}, u32[]{:S(2)}, u32[]{:S(2)}) async-start(bf16[8,2,192]{2,1,0:T(2,128)(2,1)} %reshape.402), calls=%async_computation.1 | async-start | bytes 16384 | tf_op jit(solution)/shard_map/all_to_all | solution.py:61
  65.8 0.1 reshape.401
  65.9 0.1 fusion.36
  66.0 6.3 %all-to-all-done.1 = bf16[8,2,192]{2,1,0:T(2,128)(2,1)S(1)} async-done(((bf16[8,2,192]{2,1,0:T(2,128)(2,1)}), bf16[8,2,192]{2,1,0:T(2,128)(2,1)S(1)}, u32[]{:S(2)}, u32[]{:S(2)}) %all-to-all-start.1) | async-done | bytes 6176 | tf_op jit(solution)/shard_map/all_to_all | solution.py:61
  72.3 3.3 %all-to-all-start.2 = ((bf16[8,2,192]{2,1,0:T(2,128)(2,1)}), bf16[8,2,192]{2,1,0:T(2,128)(2,1)S(1)}, u32[]{:S(2)}, u32[]{:S(2)}) async-start(bf16[8,2,192]{2,1,0:T(2,128)(2,1)} %reshape.398), calls=%async_computation.2 | async-start | bytes 16384 | tf_op jit(solution)/shard_map/all_to_all | solution.py:59
  75.6 0.1 reshape.403
  75.8 6.3 %all-to-all-done.2 = bf16[8,2,192]{2,1,0:T(2,128)(2,1)S(1)} async-done(((bf16[8,2,192]{2,1,0:T(2,128)(2,1)}), bf16[8,2,192]{2,1,0:T(2,128)(2,1)S(1)}, u32[]{:S(2)}, u32[]{:S(2)}) %all-to-all-start.2) | async-done | bytes 6176 | tf_op jit(solution)/shard_map/all_to_all | solution.py:59
  82.1 3.3 %all-to-all-start.3 = ((bf16[8,2,192]{2,1,0:T(2,128)(2,1)}), bf16[8,2,192]{2,1,0:T(2,128)(2,1)S(1)}, u32[]{:S(2)}, u32[]{:S(2)}) async-start(bf16[8,2,192]{2,1,0:T(2,128)(2,1)} %reshape.396), calls=%async_computation.3 | async-start | bytes 16384 | tf_op jit(solution)/shard_map/all_to_all | solution.py:62
  85.5 0.1 reshape.399
  85.6 0.1 fusion.37
  85.8 2.9 %fusion.5 = f32[24,1,128]{2,1,0:T(1,128)S(1)} fusion(f32[24,128,1]{1,2,0:T(1,128)S(1)} %bitcast.127, f32[1,24,128,128]{3,2,1,0:T(8,128)} %param.18), kind=kOutput, calls=%fused_computation.7 | convolution fusion | flops 4718592 | bytes 1597440 | tf_op jit(solution)/shard_map/bhkv,bhk->bhv/dot_general | solution.py:77
  88.8 0.6 multiply_add_fusion
  89.5 1.1 copy-done.2
  90.5 1.4 fusion.3
  92.0 0.1 multiply_reduce_fusion.1
  92.1 0.1 reshape.397
  92.3 0.7 reduce.8
  93.1 12.2 %all_to_all.65 = bf16[8,2,192]{2,1,0:T(2,128)(2,1)S(1)} all-to-all(bf16[8,2,192]{2,1,0:T(2,128)(2,1)S(1)} %reshape.404), channel_id=1, replica_groups=mesh['dp'=2,'kv'=8,'tp'=2] {'kv'}, dimensions={0} | all-to-all | bytes 12288 | tf_op jit(solution)/shard_map/all_to_all | solution.py:90
  105.3 0.1 reshape.405
  105.4 1.1 fusion.40
  106.5 67.6 %all-reduce.2.cloned.1.call-done = f32[8,3072]{1,0:T(8,128)} async-done(((f32[8,3072]{1,0:T(8,128)}), f32[8,3072]{1,0:T(8,128)}) %all-reduce.2.cloned.1.call-update) | async-done | bytes 98320 | tf_op jit(solution)/shard_map/psum | solution.py:92
  174.1 0.9 fusion.25
  175.0 0.1 multiply_reduce_fusion
  175.2 4.6 %convolution_multiply_fusion.1 = f32[8,1056]{1,0:T(8,128)S(1)} fusion(bf16[3072,1056]{0,1:T(8,128)(2,1)} %param.31, f32[3072]{0:T(1024)S(1)} %copy-done.7, bf16[8,3072]{1,0:T(8,128)(2,1)S(1)} %fusion.25, f32[8]{0:T(128)S(1)} %add_rsqrt_fusion), kind=kOutput, calls=%fused_computation.2 | convolution fusion | flops 51986688 | bytes 6583328 | tf_op jit(solution)/shard_map/dot_general | solution.py:97
  179.8 4.6 %fusion.2 = bf16[1,1056,8]{1,2,0:T(8,128)(2,1)S(1)} fusion(bf16[3072,1056]{0,1:T(8,128)(2,1)} %param.32, f32[3072]{0:T(1024)S(1)} %copy-done.7, bf16[8,3072]{1,0:T(8,128)(2,1)S(1)} %fusion.25, f32[8,1056]{1,0:T(8,128)S(1)} %convolution_multiply_fusion.1, f32[8]{0:T(128)S(1)} %add_rsqrt_fusion), kind=kOutput, calls=%fused_computation.4 | convolution fusion | flops 52037376 | bytes 6600224 | tf_op jit(solution)/shard_map/dot_general | solution.py:98
  184.4 30.7 %all-gather = bf16[8,1056,8]{1,2,0:T(8,128)(2,1)S(1)} all-gather(bf16[1,1056,8]{1,2,0:T(8,128)(2,1)S(1)} %fusion.2), channel_id=1, replica_groups=mesh['dp'=2,'kv'=8,'tp'=2] {'kv'}, dimensions={0}, use_global_device_ids=true | all-gather | bytes 152064 | tf_op jit(solution)/shard_map/all_gather | solution.py:102
  215.1 0.1 reshape.385
  215.3 4.4 %fusion.11 = bf16[8,384]{1,0:T(8,128)(2,1)} fusion(bf16[8448,8]{0,1:T(8,128)(2,1)S(1)} %reshape.385, bf16[8448,384]{1,0:T(8,128)(2,1)} %param.33, f32[8,3072]{1,0:T(8,128)S(1)} %convert_element_type.150, s32[]{:T(128)S(6)} %select_n.14), kind=kOutput, calls=%fused_computation.19 | convolution fusion | flops 51910656 | bytes 6641668 | tf_op jit(solution)/shard_map/dot_general | solution.py:101
  (41 shorter events, 0.6 us)
Async XLA Ops:
  7.2 98.2 %copy-start = (bf16[384,3072]{1,0:T(8,128)(2,1)S(1)}, bf16[384,3072]{1,0:T(8,128)(2,1)}, u32[]{:S(2)}) copy-start(bf16[384,3072]{1,0:T(8,128)(2,1)} %param.29) | copy-start | bytes 7077892
  44.9 14.9 %all-to-all-start = ((bf16[8,2,192]{2,1,0:T(2,128)(2,1)}), bf16[8,2,192]{2,1,0:T(2,128)(2,1)S(1)}, u32[]{:S(2)}, u32[]{:S(2)}) async-start(bf16[8,2,192]{2,1,0:T(2,128)(2,1)} %reshape.400), calls=%async_computation | async-start | bytes 16384 | tf_op jit(solution)/shard_map/all_to_all | solution.py:60
  50.3 2.8 %copy-start.3 = (bf16[3072,384]{1,0:T(8,128)(2,1)S(1)}, bf16[3072,384]{1,0:T(8,128)(2,1)}, u32[]{:S(2)}) copy-start(bf16[3072,384]{1,0:T(8,128)(2,1)} %param.20) | copy-start | bytes 7077892
  50.9 2.7 %copy-start.4 = (bf16[3072,384]{1,0:T(8,128)(2,1)S(1)}, bf16[3072,384]{1,0:T(8,128)(2,1)}, u32[]{:S(2)}) copy-start(bf16[3072,384]{1,0:T(8,128)(2,1)} %param.23) | copy-start | bytes 7077892
  53.1 1.0 copy-start.5
  53.1 1.0 copy-start.8
  53.1 1.0 copy-start.9
  53.1 1.8 copy-start.6
  59.8 12.5 %all-to-all-start.1 = ((bf16[8,2,192]{2,1,0:T(2,128)(2,1)}), bf16[8,2,192]{2,1,0:T(2,128)(2,1)S(1)}, u32[]{:S(2)}, u32[]{:S(2)}) async-start(bf16[8,2,192]{2,1,0:T(2,128)(2,1)} %reshape.402), calls=%async_computation.1 | async-start | bytes 16384 | tf_op jit(solution)/shard_map/all_to_all | solution.py:61
  72.3 9.8 %all-to-all-start.2 = ((bf16[8,2,192]{2,1,0:T(2,128)(2,1)}), bf16[8,2,192]{2,1,0:T(2,128)(2,1)S(1)}, u32[]{:S(2)}, u32[]{:S(2)}) async-start(bf16[8,2,192]{2,1,0:T(2,128)(2,1)} %reshape.398), calls=%async_computation.2 | async-start | bytes 16384 | tf_op jit(solution)/shard_map/all_to_all | solution.py:59
  82.1 10.0 %all-to-all-start.3 = ((bf16[8,2,192]{2,1,0:T(2,128)(2,1)}), bf16[8,2,192]{2,1,0:T(2,128)(2,1)S(1)}, u32[]{:S(2)}, u32[]{:S(2)}) async-start(bf16[8,2,192]{2,1,0:T(2,128)(2,1)} %reshape.396), calls=%async_computation.3 | async-start | bytes 16384 | tf_op jit(solution)/shard_map/all_to_all | solution.py:62
  85.4 88.6 %all-reduce.2.cloned.1.call-start = ((), (), s32[]{:S(2)}) async-start(), calls=%async_computation.5 | async-start | bytes 196608 | tf_op jit(solution)/shard_map/psum | solution.py:92
  85.6 3.2 %copy-start.1 = (f32[1,24,128,128]{3,2,1,0:T(8,128)S(1)}, f32[1,24,128,128]{3,2,1,0:T(8,128)}, u32[]{:S(2)}) copy-start(f32[1,24,128,128]{3,2,1,0:T(8,128)} %param.18) | copy-start | bytes 4718596
  88.8 3.4 %copy-start.10 = (f32[128]{0:T(128)S(1)}, f32[128]{0:T(128)}, u32[]{:S(2)}) copy-start(f32[128]{0:T(128)} %param.28) | copy-start | bytes 1540
  89.4 1.1 copy-start.2
  90.5 84.6 %copy-start.7 = (f32[3072]{0:T(1024)S(1)}, f32[3072]{0:T(1024)}, u32[]{:S(2)}) copy-start(f32[3072]{0:T(1024)} %param.30) | copy-start | bytes 36868
Sparse Core Ops, SparseCore 0:
  106.6 67.4 all-reduce.1
where the time goes:
time: 227 us
  waiting for transfers between devices  80.3 us (35%)
  blocking collectives  75.8 us (33%)
  matrix products  25.8 us (11%)
  starting transfers between devices  18.1 us (8%)
  between operations  14.3 us (6%)
  other arithmetic  6.49 us (3%)
  local copies, waits for them, and re-layouts  5.82 us (3%)
    psum x1, waiting for transfers between devices, body(): mixer_out = lax.psum(partial_out, 'kv')  67.6 us
    all_gather x1, blocking collectives, body(): complete_rows = lax.all_gather(tokens, 'kv', axis=1, tiled=True)  32.9 us
    all_gather x1, blocking collectives, body(): lax.all_gather(hidden_units, 'kv', axis=1, tiled=True)  30.7 us
    all_to_all x1, blocking collectives, body(): lax.all_to_all(gated_read, 'kv', split_axis=1, concat_axis=0, tiled=True)  12.2 us
    all_to_all x1, waiting for transfers between devices, body(): lax.all_to_all(query_cols, 'kv', split_axis=0, concat_axis=1, tiled=True)  6.33 us
    all_to_all x1, waiting for transfers between devices, body(): lax.all_to_all(value_cols, 'kv', split_axis=0, concat_axis=1, tiled=True)  6.29 us
    all_to_all x1, starting transfers between devices, body(): lax.all_to_all(value_cols, 'kv', split_axis=0, concat_axis=1, tiled=True)  5.99 us
    all_to_all x1, starting transfers between devices, body(): lax.all_to_all(key_cols, 'kv', split_axis=0, concat_axis=1, tiled=True)  5.36 us
  transfers between devices with their start and end apart: 5, of which 3 were waited for; matrix products, arithmetic and copies ran while one was open for 7% of the time, Pallas kernels for 0%

commit v1 on v0

--- a/solution.py
+++ b/solution.py
@@ -1,7 +1,15 @@
+import functools
+
 import jax
 import jax.numpy as jnp
 from jax import lax
+from jax.experimental import pallas as pl
+from jax.experimental.pallas import tpu as pltpu
 from jax.sharding import PartitionSpec as P
+
+MESH = pl.DeviceIdType.MESH
+F32 = jnp.float32
+BF16 = jnp.bfloat16
 
 HEADS = 24
 HEAD_DIM = 128
@@ -107,6 +115,412 @@
     return (mixed, new_state)
 
 
+TOKENS, PRE, READ, PARTIAL, RESIDUAL, HIDDEN = range(6)
+
+
+def silu(values):
+    return values / (1.0 + jnp.exp(-values))
+
+
+def layer_kernel(
+    n,
+    depth_tile,
+    tok_ref,
+    mixer_gain_ref,
+    decay_log_ref,
+    decay_bias_ref,
+    head_gain_ref,
+    channel_gain_ref,
+    w_query,
+    w_key,
+    w_value,
+    w_outgate,
+    w_decay,
+    w_write,
+    old_state,
+    w_output,
+    w_gate,
+    w_up,
+    w_down,
+    mixed_ref,
+    new_state,
+    v_query,
+    v_key,
+    v_value,
+    v_outgate,
+    v_decay,
+    v_write,
+    v_state,
+    v_output,
+    v_gate,
+    v_up,
+    v_down,
+    tok_all,
+    normed,
+    small,
+    pre_out,
+    pre_in,
+    head_rows,
+    head_vals,
+    head_gate,
+    read_rows,
+    read_out,
+    read_in,
+    part_out,
+    part_in,
+    res_own,
+    res_all,
+    hid_own,
+    hid_all,
+    sem_proj,
+    sem_small,
+    sem_mix,
+    sem_down,
+    send_sem,
+    recv_sem,
+):
+    me = lax.axis_index("kv")
+    rows, share = tok_ref.shape
+    local_rows, heads = v_state.shape[0], v_state.shape[1]
+    width = n * share
+    own_heads = share // HEAD_DIM
+    hidden_share = v_gate.shape[1]
+    steps = width // depth_tile
+
+    barrier = pltpu.get_barrier_semaphore()
+    for k in range(1, n):
+        pl.semaphore_signal(
+            barrier, inc=1, device_id={"kv": lax.rem(me + k, n)}, device_id_type=MESH
+        )
+
+    proj = ((w_query, v_query), (w_key, v_key), (w_value, v_value), (w_outgate, v_outgate))
+    mix = ((w_gate, v_gate), (w_up, v_up))
+
+    def tile_copy(pair, step, sem):
+        part = pl.ds(pl.multiple_of(step * depth_tile, depth_tile), depth_tile)
+        return pltpu.make_async_copy(pair[0].at[part], pair[1].at[part], sem)
+
+    def proj_copy(which, step):
+        return tile_copy(proj[which], step, sem_proj.at[step, which])
+
+    def mix_copy(which, step):
+        return tile_copy(mix[which], step, sem_mix.at[step, which])
+
+    def down_copy(step):
+        part = pl.ds(pl.multiple_of(step * hidden_share, 16), hidden_share)
+        return pltpu.make_async_copy(w_down.at[part], v_down.at[part], sem_down.at[step])
+
+    decay_copy = pltpu.make_async_copy(w_decay, v_decay, sem_small.at[0])
+    write_copy = pltpu.make_async_copy(w_write, v_write, sem_small.at[1])
+    state_copy = pltpu.make_async_copy(old_state, v_state, sem_small.at[2])
+    output_copy = pltpu.make_async_copy(w_output, v_output, sem_small.at[3])
+    decay_copy.start()
+    write_copy.start()
+    for step in range(steps):
+        for which in range(4):
+            proj_copy(which, step).start()
+
+    pl.semaphore_wait(barrier, n - 1)
+
+    def exchange(phase, source, slots):
+        copies = []
+        for k in range(1, n):
+            peer = lax.rem(me + k, n)
+            copy = pltpu.make_async_remote_copy(
+                src_ref=source(peer),
+                dst_ref=slots.at[me],
+                send_sem=send_sem.at[phase, k],
+                recv_sem=recv_sem.at[phase, k],
+                device_id={"kv": peer},
+                device_id_type=MESH,
+            )
+            copy.start()
+            copies.append(copy)
+        return copies
+
+    def arrive(copies):
+        for copy in copies:
+            copy.wait_recv()
+
+    all_copies = []
+
+    copies = exchange(TOKENS, lambda peer: tok_ref, tok_all)
+    all_copies += copies
+    state_copy.start()
+    output_copy.start()
+    for step in range(steps):
+        for which in range(2):
+            mix_copy(which, step).start()
+    for step in range(n):
+        down_copy(step).start()
+    tok_all[me] = tok_ref[...]
+    if pre_out.shape[1] > 4 * own_heads:
+        pre_out[:, 4 * own_heads :, :] = jnp.zeros(
+            (rows, pre_out.shape[1] - 4 * own_heads, HEAD_DIM), F32
+        )
+    read_out[...] = jnp.zeros_like(read_out)
+    head_rows[...] = jnp.zeros_like(head_rows)
+    arrive(copies)
+
+    def norm_into(blocks, gain_ref):
+        squares = jnp.zeros((rows, 1), F32)
+        for s in range(n):
+            cols = slice(s * share, (s + 1) * share)
+            wide = blocks[s].astype(F32)
+            squares += jnp.sum(wide * wide, axis=-1, keepdims=True)
+            normed[:, cols] = (wide * gain_ref[:, cols]).astype(BF16)
+        return lax.rsqrt(squares / width + EPS)
+
+    scale_in = norm_into(tok_all, mixer_gain_ref)
+
+    decay_copy.wait()
+    write_copy.wait()
+
+    def proj_step(step, sums):
+        part = pl.ds(pl.multiple_of(step * depth_tile, depth_tile), depth_tile)
+        lhs = normed[:, part]
+        out = []
+        for which in range(4):
+            proj_copy(which, step).wait()
+            out.append(
+                sums[which]
+                + jnp.dot(lhs, proj[which][1][part, :], preferred_element_type=F32)
+            )
+        out.append(sums[4] + jnp.dot(lhs, v_decay[part, :], preferred_element_type=F32))
+        out.append(sums[5] + jnp.dot(lhs, v_write[part, :], preferred_element_type=F32))
+        return tuple(out)
+
+    zeros = lambda cols: jnp.zeros((rows, cols), F32)
+    sums = lax.fori_loop(
+        0, steps, proj_step, (zeros(share),) * 4 + (zeros(heads),) * 2
+    )
+    for which in range(4):
+        pre = (sums[which] * scale_in).astype(BF16).astype(F32)
+        for j in range(own_heads):
+            pre_out[:, which * own_heads + j, :] = pre[:, j * HEAD_DIM : (j + 1) * HEAD_DIM]
+
+    def row_block(peer):
+        return pre_out.at[pl.ds(peer * local_rows, local_rows)]
+
+    copies = exchange(PRE, row_block, pre_in)
+    all_copies += copies
+    pre_in[me] = pre_out[pl.ds(me * local_rows, local_rows)]
+    small[0] = sums[4] * scale_in
+    small[1] = sums[5] * scale_in
+    state_copy.wait()
+    arrive(copies)
+
+    for l in range(local_rows):
+        own = pl.ds(me * local_rows + l, 1)
+        decay_pre = small[0, own, :]
+        write_pre = small[1, own, :]
+        strength = 1.0 / (1.0 + jnp.exp(-write_pre))
+        shifted = decay_pre + decay_bias_ref[...]
+        softplus = jnp.maximum(shifted, 0.0) + jnp.log1p(jnp.exp(-jnp.abs(shifted)))
+        retain = jnp.exp(-jnp.exp(decay_log_ref[...]) * softplus)
+        for s in range(n):
+            act = silu(pre_in[s, l])
+            unit = act * lax.rsqrt(jnp.sum(act * act, axis=-1, keepdims=True) + EPS)
+            at = s * own_heads
+            c = own_heads
+            head_rows[at : at + c, :] = unit[c : 2 * c]
+            head_rows[heads + at : heads + at + c, :] = unit[:c] * HEAD_DIM ** (-0.5)
+            head_vals[at : at + c, :] = act[2 * c : 3 * c]
+            head_gate[at : at + c, :] = act[3 * c : 4 * c]
+        columns = head_rows[...].T
+        for h in range(heads):
+            key = columns[:, h : h + 1]
+            query = columns[:, heads + h : heads + h + 1]
+            keep = retain[:, h : h + 1]
+            old = v_state[l, h]
+            recalled = jnp.sum(old * key, axis=0, keepdims=True)
+            correction = head_vals[h : h + 1, :] - keep * recalled
+            new = keep * old + key * (strength[:, h : h + 1] * correction)
+            v_state[l, h] = new
+            read_rows[h : h + 1, :] = jnp.sum(new * query, axis=0, keepdims=True)
+        read = read_rows[...]
+        scale = lax.rsqrt(jnp.mean(read * read, axis=-1, keepdims=True) + EPS)
+        gated = (read * scale * head_gain_ref[...] * head_gate[...]).astype(BF16).astype(F32)
+        for s in range(n):
+            read_out[s, l, :own_heads, :] = gated[s * own_heads : (s + 1) * own_heads]
+
+    copies = exchange(READ, lambda peer: read_out.at[peer], read_in)
+    all_copies += copies
+    state_out = pltpu.make_async_copy(v_state, new_state, sem_small.at[4])
+    state_out.start()
+    read_in[me] = read_out[me]
+    output_copy.wait()
+    arrive(copies)
+    read_cols = jnp.concatenate(
+        [read_in[:, :, j, :].reshape(rows, HEAD_DIM) for j in range(own_heads)], axis=1
+    ).astype(BF16)
+    for s in range(n):
+        part_out[s] = jnp.dot(
+            read_cols, v_output[:, s * share : (s + 1) * share], preferred_element_type=F32
+        )
+
+    copies = exchange(PARTIAL, lambda peer: part_out.at[peer], part_in)
+    all_copies += copies
+    part_in[me] = part_out[me]
+    arrive(copies)
+    residual = tok_ref[...].astype(F32)
+    mixer = part_in[0]
+    for s in range(1, n):
+        mixer += part_in[s]
+    res_own[...] = (residual + mixer).astype(BF16)
+    copies = exchange(RESIDUAL, lambda peer: res_own, res_all)
+    all_copies += copies
+    res_all[me] = res_own[...]
+    arrive(copies)
+    scale_mid = norm_into(res_all, channel_gain_ref)
+
+    def mix_step(step, sums):
+        part = pl.ds(pl.multiple_of(step * depth_tile, depth_tile), depth_tile)
+        lhs = normed[:, part]
+        out = []
+        for which in range(2):
+            mix_copy(which, step).wait()
+            out.append(
+                sums[which] + jnp.dot(lhs, mix[which][1][part, :], preferred_element_type=F32)
+            )
+        return tuple(out)
+
+    gate, up = lax.fori_loop(0, steps, mix_step, (zeros(hidden_share),) * 2)
+    hid_own[...] = (silu(gate * scale_mid) * (up * scale_mid)).astype(BF16)
+
+    copies = exchange(HIDDEN, lambda peer: hid_own, hid_all)
+    all_copies += copies
+    hid_all[me] = hid_own[...]
+    arrive(copies)
+
+    def down_step(step, total):
+        down_copy(step).wait()
+        part = pl.ds(pl.multiple_of(step * hidden_share, 16), hidden_share)
+        return total + jnp.dot(hid_all[step], v_down[part, :], preferred_element_type=F32)
+
+    total = lax.fori_loop(0, n, down_step, zeros(share))
+    mixed_ref[...] = (res_own[...].astype(F32) + total).astype(BF16)
+
+    for copy in all_copies:
+        copy.wait_send()
+    state_out.wait()
+
+
+def round_up(value, unit):
+    return -(-value // unit) * unit
+
+
+def fused_body(
+    n,
+    tokens,
+    old_state,
+    mixer_gain,
+    w_query,
+    w_key,
+    w_value,
+    w_outgate,
+    w_decay,
+    w_write,
+    decay_log,
+    decay_bias,
+    head_gain,
+    w_output,
+    channel_gain,
+    w_gate,
+    w_up,
+    w_down,
+):
+    rows, share = tokens.shape
+    local_rows, heads = old_state.shape[:2]
+    width, hidden_share = w_gate.shape
+    own_heads = share // HEAD_DIM
+    depth_tile = 512 if width % 512 == 0 else share
+    steps = width // depth_tile
+    pre_rows = round_up(4 * own_heads, 8)
+    read_slots = round_up(own_heads, 8)
+    vmem = pl.BlockSpec(memory_space=pltpu.VMEM)
+    hbm = pl.BlockSpec(memory_space=pl.ANY)
+    buf = pltpu.VMEM
+    sem = pltpu.SemaphoreType.DMA
+    wide = lambda vector: vector.reshape(1, -1)
+    return tuple(
+        pl.pallas_call(
+            functools.partial(layer_kernel, n, depth_tile),
+            out_shape=(
+                jax.ShapeDtypeStruct((rows, share), BF16),
+                jax.ShapeDtypeStruct(old_state.shape, F32),
+            ),
+            in_specs=[vmem] * 6 + [hbm] * 11,
+            out_specs=(vmem, hbm),
+            scratch_shapes=[
+                buf((width, share), BF16),
+                buf((width, share), BF16),
+                buf((width, share), BF16),
+                buf((width, share), BF16),
+                buf(w_decay.shape, BF16),
+                buf(w_write.shape, BF16),
+                buf(old_state.shape, F32),
+                buf(w_output.shape, BF16),
+                buf(w_gate.shape, BF16),
+                buf(w_up.shape, BF16),
+                buf(w_down.shape, BF16),
+                buf((n, rows, share), BF16),
+                buf((rows, width), BF16),
+                buf((2, rows, heads), F32),
+                buf((rows, pre_rows, HEAD_DIM), F32),
+                buf((n, local_rows, pre_rows, HEAD_DIM), F32),
+                buf((round_up(2 * heads, 128), HEAD_DIM), F32),
+                buf((heads, HEAD_DIM), F32),
+                buf((heads, HEAD_DIM), F32),
+                buf((heads, HEAD_DIM), F32),
+                buf((n, local_rows, read_slots, HEAD_DIM), F32),
+                buf((n, local_rows, read_slots, HEAD_DIM), F32),
+                buf((n, rows, share), F32),
+                buf((n, rows, share), F32),
+                buf((rows, share), BF16),
+                buf((n, rows, share), BF16),
+                buf((rows, hidden_share), BF16),
+                buf((n, rows, hidden_share), BF16),
+                sem((steps, 4)),
+                sem((5,)),
+                sem((steps, 2)),
+                sem((n,)),
+                sem((6, n)),
+                sem((6, n)),
+            ],
+            compiler_params=pltpu.CompilerParams(
+                collective_id=0, has_side_effects=True, vmem_limit_bytes=63 * 2**20
+            ),
+        )(
+            tokens,
+            wide(mixer_gain),
+            wide(decay_log),
+            wide(decay_bias),
+            wide(head_gain),
+            wide(channel_gain),
+            w_query,
+            w_key,
+            w_value,
+            w_outgate,
+            w_decay,
+            w_write,
+            old_state,
+            w_output,
+            w_gate,
+            w_up,
+            w_down,
+        )
+    )
+
+
+def any_body(n, tokens, old_state, *rest):
+    whole_heads = tokens.shape[1] % HEAD_DIM == 0 and tokens.shape[0] % 8 == 0
+    held = sum(a.size * a.dtype.itemsize for a in (old_state, *rest))
+    if whole_heads and held < 40 * 2**20:
+        return fused_body(n, tokens, old_state, *rest)
+    return body(tokens, old_state, *rest)
+
+
 def solution(mesh):
     in_specs = (
         P(("tp", "dp"), "kv"),
@@ -128,4 +542,5 @@
         P(None, "kv"),
     )
     out_specs = (P(("tp", "dp"), "kv"), P(("tp", "dp", "kv"), None, None, None))
-    return jax.shard_map(body, mesh=mesh, in_specs=in_specs, out_specs=out_specs, check_vma=False)
+    return jax.shard_map(
+        functools.partial(any_body, mesh.shape["kv"]), mesh=mesh, in_specs=in_specs, out_specs=out_specs, check_vma=False)

time: 227 us -> 73.6 us (0.32)
  waiting for transfers between devices: 80.3 us -> 0 us
  blocking collectives: 75.8 us -> 0 us
  Pallas kernels: 0 us -> 45.5 us
  matrix products: 25.8 us -> 0 us
  local copies, waits for them, and re-layouts: 5.82 us -> 26.8 us
  starting transfers between devices: 18.1 us -> 0 us
  between operations: 14.3 us -> 0.64 us
  other arithmetic: 6.49 us -> 0 us
    psum x1 -> x0, waiting for transfers between devices: 67.6 us -> none  [body(): mixer_out = lax.psum(partial_out, 'kv')]
    all_gather x2 -> x0, blocking collectives: 63.6 us -> none  [the longest x1 32.9 us: body(): complete_rows = lax.all_gather(tokens, 'kv', axis=1, tiled=True)]
    pallas_call x0 -> x1, Pallas kernels: none -> 45.5 us  [fused_body(): pl.pallas_call(functools.partial(layer_kernel, n, depth_tile), out_shape=...]
    dot_general x12 -> x0, matrix products: 25.8 us -> none  [the longest x4 5.09 us: project(): jnp.dot(normed, weight, preferred_element_type=jnp.float32) * scale_in]
    unnamed x33 -> x6, local copies, waits for them, and re-layouts: 4.66 us -> 26.8 us
    all_to_all x4 -> x0, starting transfers between devices: 18 us -> none  [the longest x1 5.99 us: body(): lax.all_to_all(value_cols, 'kv', split_axis=0, concat_axis=1, tiled=True)]
    all_to_all x4 -> x0, waiting for transfers between devices: 12.6 us -> none  [the longest x1 6.33 us: body(): lax.all_to_all(query_cols, 'kv', split_axis=0, concat_axis=1, tiled=True)]
    all_to_all x1 -> x0, blocking collectives: 12.2 us -> none  [body(): lax.all_to_all(gated_read, 'kv', split_axis=1, concat_axis=0, tiled=True)]
  transfers between devices with their start and end apart: 5 -> 0, of which waited for: 3 -> 0; matrix products, arithmetic and copies ran while one was open for 7% -> 0% of each run, Pallas kernels for 0% -> 0%
where the time goes in v1:
time: 73.6 us; the launch traced here: 72.9 us
  Pallas kernels  45.5 us (62%)
  local copies, waits for them, and re-layouts  26.8 us (36%)
    pallas_call x1, Pallas kernels, fused_body(): pl.pallas_call(functools.partial(layer_kernel, n, depth_tile), out_shape=...  45.5 us
    unnamed x6, local copies, waits for them, and re-layouts  26.8 us

profile of v1, /device:TPU:0, one launch (start us, length us, event | category | flops | bytes accessed | tf_op | source)
XLA Modules:
  0.0 72.9 jit_solution(15046085116545538323)
XLA Ops:
  0.6 2.1 %copy.19.w_decay = bf16[3072,24]{1,0:T(8,128)(2,1)} copy(bf16[3072,24]{0,1:T(8,128)(2,1)} %param.24) | data formatting | bytes 294912 | tf_op args[7]
  2.7 2.1 %copy.20.w_write = bf16[3072,24]{1,0:T(8,128)(2,1)} copy(bf16[3072,24]{0,1:T(8,128)(2,1)} %param.25) | data formatting | bytes 294912 | tf_op args[8]
  4.8 9.3 %copy.21.w_gate = bf16[3072,1056]{1,0:T(8,128)(2,1)} copy(bf16[3072,1056]{0,1:T(8,128)(2,1)} %param.31) | data formatting | bytes 12976128 | tf_op args[14]
  14.1 9.3 %copy.22.w_up = bf16[3072,1056]{1,0:T(8,128)(2,1)} copy(bf16[3072,1056]{0,1:T(8,128)(2,1)} %param.32) | data formatting | bytes 12976128 | tf_op args[15]
  23.4 45.5 %shard_map.176 = (bf16[8,384]{1,0:T(8,128)(2,1)}, f32[1,24,128,128]{3,2,1,0:T(8,128)}) custom-call(bf16[8,384]{1,0:T(8,128)(2,1)} %tok_ref.1, f32[1,3072]{1,0:T(1,128)} %bitcast.5, f32[1,24]{1,0:T(1,128)} %bitcast.7, f32[1,24]{1,0:T(1,128)} %bitcast.8, f32[1,128]{1,0:T(1,128)} %bitcast.9, f32[1,3072]{1,0:T(1,128)} %bitcast.6, bf16[3072,384]{1,0:T(8,128)(2,1)} %w_query.1, ...), custom_call_target="tpu_custom_call" | custom-call | tf_op jit(solution)/shard_map/pallas_call | solution.py:447
  68.9 1.3 %copy.25 = bf16[8,384]{1,0:T(8,128)(2,1)} copy(bf16[8,384]{1,0:T(8,128)(2,1)} %get-tuple-element.4) | data formatting | bytes 12288
  70.2 2.7 %copy.26 = f32[1,24,128,128]{3,2,1,0:T(8,128)} copy(f32[1,24,128,128]{3,2,1,0:T(8,128)} %get-tuple-element.5) | data formatting | bytes 3145728

commit v2 on v1

--- a/solution.py
+++ b/solution.py
@@ -120,6 +120,10 @@
 
 def silu(values):
     return values / (1.0 + jnp.exp(-values))
+
+
+def dot_rows(lhs, rows):
+    return lax.dot_general(lhs, rows, (((1,), (1,)), ((), ())), preferred_element_type=F32)
 
 
 def layer_kernel(
@@ -184,7 +188,7 @@
     local_rows, heads = v_state.shape[0], v_state.shape[1]
     width = n * share
     own_heads = share // HEAD_DIM
-    hidden_share = v_gate.shape[1]
+    hidden_share = v_gate.shape[0]
     steps = width // depth_tile
 
     barrier = pltpu.get_barrier_semaphore()
@@ -204,7 +208,10 @@
         return tile_copy(proj[which], step, sem_proj.at[step, which])
 
     def mix_copy(which, step):
-        return tile_copy(mix[which], step, sem_mix.at[step, which])
+        part = pl.ds(pl.multiple_of(step * depth_tile, depth_tile), depth_tile)
+        return pltpu.make_async_copy(
+            mix[which][0].at[:, part], mix[which][1].at[:, part], sem_mix.at[step, which]
+        )
 
     def down_copy(step):
         part = pl.ds(pl.multiple_of(step * hidden_share, 16), hidden_share)
@@ -286,8 +293,8 @@
                 sums[which]
                 + jnp.dot(lhs, proj[which][1][part, :], preferred_element_type=F32)
             )
-        out.append(sums[4] + jnp.dot(lhs, v_decay[part, :], preferred_element_type=F32))
-        out.append(sums[5] + jnp.dot(lhs, v_write[part, :], preferred_element_type=F32))
+        out.append(sums[4] + dot_rows(lhs, v_decay[:, part]))
+        out.append(sums[5] + dot_rows(lhs, v_write[:, part]))
         return tuple(out)
 
     zeros = lambda cols: jnp.zeros((rows, cols), F32)
@@ -381,7 +388,7 @@
         for which in range(2):
             mix_copy(which, step).wait()
             out.append(
-                sums[which] + jnp.dot(lhs, mix[which][1][part, :], preferred_element_type=F32)
+                sums[which] + dot_rows(lhs, mix[which][1][:, part])
             )
         return tuple(out)
 
@@ -457,12 +464,12 @@
                 buf((width, share), BF16),
                 buf((width, share), BF16),
                 buf((width, share), BF16),
-                buf(w_decay.shape, BF16),
-                buf(w_write.shape, BF16),
+                buf((heads, width), BF16),
+                buf((heads, width), BF16),
                 buf(old_state.shape, F32),
                 buf(w_output.shape, BF16),
-                buf(w_gate.shape, BF16),
-                buf(w_up.shape, BF16),
+                buf((hidden_share, width), BF16),
+                buf((hidden_share, width), BF16),
                 buf(w_down.shape, BF16),
                 buf((n, rows, share), BF16),
                 buf((rows, width), BF16),
@@ -502,12 +509,12 @@
             w_key,
             w_value,
             w_outgate,
-            w_decay,
-            w_write,
+            w_decay.T,
+            w_write.T,
             old_state,
             w_output,
-            w_gate,
-            w_up,
+            w_gate.T,
+            w_up.T,
             w_down,
         )
     )

time: 73.6 us -> 51.8 us (0.70)
  local copies, waits for them, and re-layouts: 26.8 us -> 3.99 us
  Pallas kernels: 45.5 us -> 46.9 us
    unnamed x6 -> x2, local copies, waits for them, and re-layouts: 26.8 us -> 3.99 us
    pallas_call x1, Pallas kernels: 45.5 us -> 46.9 us  [fused_body(): pl.pallas_call(functools.partial(layer_kernel, n, depth_tile), out_shape=...]
where the time goes in v2:
time: 51.8 us; the launch traced here: 51.5 us
  Pallas kernels  46.9 us (91%)
  local copies, waits for them, and re-layouts  3.99 us (8%)
  between operations  0.65 us (1%)
    pallas_call x1, Pallas kernels, fused_body(): pl.pallas_call(functools.partial(layer_kernel, n, depth_tile), out_shape=...  46.9 us
    unnamed x2, local copies, waits for them, and re-layouts  3.99 us

profile of v2, /device:TPU:0, one launch (start us, length us, event | category | flops | bytes accessed | tf_op | source)
XLA Modules:
  0.0 51.5 jit_solution(8946760344731177188)
XLA Ops:
  0.6 46.9 %shard_map.176 = (bf16[8,384]{1,0:T(8,128)(2,1)}, f32[1,24,128,128]{3,2,1,0:T(8,128)}) custom-call(bf16[8,384]{1,0:T(8,128)(2,1)} %tok_ref.1, f32[1,3072]{1,0:T(1,128)} %bitcast.13, f32[1,24]{1,0:T(1,128)} %bitcast.15, f32[1,24]{1,0:T(1,128)} %bitcast.16, f32[1,128]{1,0:T(1,128)} %bitcast.17, f32[1,3072]{1,0:T(1,128)} %bitcast.14, ...), custom_call_target="tpu_custom_call" | custom-call | tf_op jit(solution)/shard_map/pallas_call | solution.py:454
  47.5 1.3 %copy.21 = bf16[8,384]{1,0:T(8,128)(2,1)} copy(bf16[8,384]{1,0:T(8,128)(2,1)} %get-tuple-element.4) | data formatting | bytes 12288
  48.8 2.7 %copy.22 = f32[1,24,128,128]{3,2,1,0:T(8,128)} copy(f32[1,24,128,128]{3,2,1,0:T(8,128)} %get-tuple-element.5) | data formatting | bytes 3145728
